TPU v7x, 32 devices: a whole 2x2x4 slice. The times are simulated.
32 devices in a mesh: ep: 8 (over z, x), tp: 4 (over y, core).
Axes of the slice: x: 2, y: 2, z: 4, core: 2. Of those that a mesh axis runs over, the one named last changes fastest.
Arguments:
- hidden_in: bfloat16 [256, 4096], P('ep'), may hold values from -6 to 6
- norm_gain: float32 [4096], replicated, may hold values from 0.1 to 1.9
- group_ids: int32 [256], P('ep'), may hold values from 0 to 1, as said below
- inner_ids: int32 [256, 4], P('ep'), may hold values from 0 to 7, as said below
- group_prob: float32 [256], P('ep'), may hold values from 0.25 to 1
- expert_prob: float32 [256, 4], P('ep'), may hold values from 0.1 to 1
- w_gate: bfloat16 [16, 4096, 1024], P('ep', None, 'tp'), may hold values from -0.09375 to 0.09375
- w_up: bfloat16 [16, 4096, 1024], P('ep', None, 'tp'), may hold values from -0.09375 to 0.09375
- w_down: bfloat16 [16, 1024, 4096], P('ep', None, 'tp'), may hold values from -0.1875 to 0.1875
Outputs:
- moe_out: bfloat16 [256, 4096], P('ep', 'tp')
Inputs may be any that keep to these rules, and one draw needn't show every extreme that they name: `group_ids`: among the 32 tokens of one index of ep no group is named by more than 16 tokens; one group is named by exactly 16 of them, and all of these name one common expert of it. `inner_ids`: each row names 4 different experts of the token's group.
All inputs are finite; a program needn't handle non-finite values.
Results may differ from a plain program's by a relative error of at most 0.0069.
Values may be sent and summed in bfloat16 or wider, within the bound.
No kernel may reach another device: no remote copies, remote signals or barrier semaphores. Data moves between devices by JAX's collectives and lax.ppermute only.
A program may use at most 64 MiB of HBM per device.

v0:
```python
import jax
import jax.numpy as jnp
from jax import lax
from jax.sharding import PartitionSpec as P

EPG = 8


EPS = 1e-06


def expert_block(token_rows, weights, w_gate, w_up, w_down):
    gate_proj = jnp.einsum("rd,edh->erh", token_rows, w_gate, preferred_element_type=jnp.float32)
    up_proj = jnp.einsum("rd,edh->erh", token_rows, w_up, preferred_element_type=jnp.float32)
    activation = (jax.nn.silu(gate_proj) * up_proj * weights.T[:, :, None]).astype(jnp.bfloat16)
    return jnp.einsum(
        "erh,ehd->rd",
        lax.all_gather(activation, "tp", axis=2, tiled=True),
        w_down,
        preferred_element_type=jnp.float32,
    )


def on_device(
    hidden_in, norm_gain, group_ids, inner_ids, group_prob, expert_prob, w_gate, w_up, w_down
):
    widened = hidden_in.astype(jnp.float32)
    normed = (
        widened * lax.rsqrt(jnp.mean(widened * widened, axis=-1, keepdims=True) + EPS) * norm_gain
    ).astype(jnp.bfloat16)
    ep_count = lax.axis_size("ep")
    local_count = w_gate.shape[0]
    expert_count = local_count * ep_count
    tok_rows = normed.shape[0]
    expert_ids = group_ids[:, None] * EPG + inner_ids
    scaled = group_prob[:, None] * expert_prob
    matches = (expert_ids[:, :, None] == jnp.arange(expert_count)[None, None, :]).astype(
        jnp.float32
    )
    route_dense = jnp.sum(matches * scaled[:, :, None], axis=1)
    capacity = tok_rows // 2
    owners = expert_ids // local_count
    routed = jnp.any(owners[:, :, None] == jnp.arange(ep_count)[None, None, :], axis=1)
    slot_index = jnp.cumsum(routed.astype(jnp.int32), axis=0) - 1
    hit_slot = slot_index.T[:, None, :] == jnp.arange(capacity)[None, :, None]
    dispatch = (routed.T[:, None, :] & hit_slot).astype(jnp.float32)
    send_rows = jnp.einsum(
        "psr,rd->psd", dispatch.astype(jnp.bfloat16), normed, preferred_element_type=jnp.float32
    ).astype(jnp.bfloat16)
    send_weights = jnp.einsum(
        "psr,rpe->pse",
        dispatch,
        route_dense.reshape(tok_rows, ep_count, local_count),
        precision=lax.Precision.HIGHEST,
    )
    got_rows = lax.all_to_all(send_rows, "ep", split_axis=0, concat_axis=0, tiled=True)
    got_weights = lax.all_to_all(send_weights, "ep", split_axis=0, concat_axis=0, tiled=True)
    partial_value = expert_block(
        got_rows.reshape(ep_count * capacity, got_rows.shape[2]),
        got_weights.reshape(ep_count * capacity, local_count),
        w_gate,
        w_up,
        w_down,
    )
    returned = lax.all_to_all(
        partial_value.reshape(ep_count, capacity, partial_value.shape[1]),
        "ep",
        split_axis=0,
        concat_axis=0,
        tiled=True,
    )
    combined = jnp.einsum("psr,psd->rd", dispatch, returned, precision=lax.Precision.HIGHEST)
    return combined.astype(jnp.bfloat16)


def solution(mesh):
    placed = (
        P("ep", None),
        P(),
        P("ep"),
        P("ep", None),
        P("ep"),
        P("ep", None),
        P("ep", None, "tp"),
        P("ep", None, "tp"),
        P("ep", None, "tp"),
    )
    return jax.shard_map(
        on_device, mesh=mesh, in_specs=placed, out_specs=P("ep", "tp"), check_vma=False
    )
```

profile of v0, /device:TPU:0, one launch (start us, length us, event | category | flops | bytes accessed | tf_op | source)
XLA Modules:
  0.0 76.7 jit_solution(13382884557020373992)
XLA Ops:
  0.0 0.7 broadcast_multiply_fusion.1
  0.7 0.7 add_select_fusion
  1.4 0.1 copy.21
  1.4 0.1 reduce_window_sum.11
  1.5 0.1 copy.22
  1.6 0.7 broadcast_multiply_fusion
  2.3 0.8 %fusion.13 = f32[8,16,2]{1,2,0:T(2,128)} fusion(f32[32,8,2]{0,2,1:T(2,128)S(1)} %bitcast.44, s32[8,32]{1,0:T(8,128)S(1)} %copy.22, pred[8,32]{1,0:T(8,128)(4,1)S(1)} %bitcast.41), kind=kOutput, calls=%fused_computation.19 | convolution fusion | flops 106496 | bytes 4352 | tf_op jit(solution)/shard_map/psr,rpe->pse/dot_general | solution.py:50
  3.1 7.3 %all-to-all-start.1 = ((f32[8,16,2]{1,2,0:T(2,128)}), f32[8,16,2]{1,2,0:T(2,128)S(1)}, u32[]{:S(2)}, u32[]{:S(2)}) async-start(f32[8,16,2]{1,2,0:T(2,128)} %fusion.13), calls=%async_computation.1 | async-start | bytes 16384 | tf_op jit(solution)/shard_map/all_to_all | solution.py:57
  10.3 1.1 %fusion.4 = f32[32]{0:T(128)S(1)} fusion(bf16[32,4096]{1,0:T(8,128)(2,1)} %param.9), kind=kLoop, calls=%fused_computation.10 | loop fusion | flops 393184 | bytes 262272 | tf_op jit(solution)/shard_map/reduce_sum | solution.py:29
  11.5 2.4 %convolution_convert_fusion = bf16[8,16,4096]{2,1,0:T(8,128)(2,1)} fusion(bf16[32,4096]{1,0:T(8,128)(2,1)} %param.9, f32[4096]{0:T(1024)} %param.10, f32[32]{0:T(128)S(1)} %add_rsqrt_fusion, s32[8,32]{1,0:T(8,128)S(1)} %copy.22, pred[8,32]{1,0:T(8,128)(4,1)S(1)} %bitcast.42), kind=kOutput, calls=%fused_computation | convolution fusion | flops 34619392 | bytes 1328512 | tf_op jit(solution)/shard_map/psr,rd->psd/dot_general | solution.py:47
  13.9 3.0 %all-to-all-done.1 = f32[8,16,2]{1,2,0:T(2,128)S(1)} async-done(((f32[8,16,2]{1,2,0:T(2,128)}), f32[8,16,2]{1,2,0:T(2,128)S(1)}, u32[]{:S(2)}, u32[]{:S(2)}) %all-to-all-start.1) | async-done | bytes 1056 | tf_op jit(solution)/shard_map/all_to_all | solution.py:57
  16.9 3.6 %all-to-all-start = ((bf16[8,16,4096]{2,1,0:T(8,128)(2,1)}), bf16[8,16,4096]{2,1,0:T(8,128)(2,1)S(1)}, u32[]{:S(2)}, u32[]{:S(2)}) async-start(bf16[8,16,4096]{2,1,0:T(8,128)(2,1)} %convolution_convert_fusion), calls=%async_computation | async-start | bytes 2097152 | tf_op jit(solution)/shard_map/all_to_all | solution.py:56
  20.4 0.1 reshape.32
  20.5 24.8 %all-to-all-done = bf16[8,16,4096]{2,1,0:T(8,128)(2,1)S(1)} async-done(((bf16[8,16,4096]{2,1,0:T(8,128)(2,1)}), bf16[8,16,4096]{2,1,0:T(8,128)(2,1)S(1)}, u32[]{:S(2)}, u32[]{:S(2)}) %all-to-all-start) | async-done | bytes 1048608 | tf_op jit(solution)/shard_map/all_to_all | solution.py:56
  45.3 0.0 copy-start.1
  45.3 3.0 %convolution_bitcast_fusion.1 = f32[2,128,256]{2,1,0:T(8,128)S(1)} fusion(bf16[128,4096,1]{1,0,2:T(8,128)(2,1)S(1)} %bitcast.38, bf16[2,4096,256]{2,1,0:T(8,128)(2,1)} %param.15), kind=kOutput, calls=%fused_computation.2 | convolution fusion | flops 536870912 | bytes 5505024 | tf_op jit(solution)/shard_map/rd,edh->erh/dot_general | solution.py:13
  48.4 0.0 copy-start
  48.4 0.4 copy-done.1
  48.8 0.8 fusion.2
  49.5 7.3 %all_gather.3 = bf16[2,128,1024]{2,1,0:T(8,128)(2,1)S(1)} all-gather(bf16[2,128,256]{2,1,0:T(8,128)(2,1)S(1)} %fusion.2), channel_id=1, replica_groups=mesh['ep'=8,'tp'=4] {'tp'}, dimensions={2}, use_global_device_ids=true | all-gather | bytes 655360 | tf_op jit(solution)/shard_map/all_gather | solution.py:18
  56.9 0.0 copy-done
  56.9 0.7 fusion.24
  57.6 18.2 %all_to_all.15 = f32[8,16,1024]{2,1,0:T(8,128)S(1)} all-to-all(f32[8,16,1024]{2,1,0:T(8,128)S(1)} %bitcast.40), channel_id=1, replica_groups=mesh['ep'=8,'tp'=4] {'ep'}, dimensions={0} | all-to-all | bytes 1048576 | tf_op jit(solution)/shard_map/all_to_all | solution.py:65
  75.8 0.9 %fusion.3 = bf16[32,1024]{1,0:T(8,128)(2,1)} fusion(f32[8,16,1024]{2,1,0:T(8,128)S(1)} %all_to_all.15, s32[8,32]{1,0:T(8,128)S(1)} %copy.22, pred[8,32]{1,0:T(8,128)(4,1)S(1)} %bitcast.43), kind=kOutput, calls=%fused_computation.7 | convolution fusion | flops 50372608 | bytes 591104 | tf_op jit(solution)/shard_map/psr,psd->rd/dot_general | solution.py:72
  (6 shorter events, 0.0 us)
Async XLA Ops:
  3.1 13.8 %all-to-all-start.1 = ((f32[8,16,2]{1,2,0:T(2,128)}), f32[8,16,2]{1,2,0:T(2,128)S(1)}, u32[]{:S(2)}, u32[]{:S(2)}) async-start(f32[8,16,2]{1,2,0:T(2,128)} %fusion.13), calls=%async_computation.1 | async-start | bytes 16384 | tf_op jit(solution)/shard_map/all_to_all | solution.py:57
  16.9 28.5 %all-to-all-start = ((bf16[8,16,4096]{2,1,0:T(8,128)(2,1)}), bf16[8,16,4096]{2,1,0:T(8,128)(2,1)S(1)}, u32[]{:S(2)}, u32[]{:S(2)}) async-start(bf16[8,16,4096]{2,1,0:T(8,128)(2,1)} %convolution_convert_fusion), calls=%async_computation | async-start | bytes 2097152 | tf_op jit(solution)/shard_map/all_to_all | solution.py:56
  45.3 3.4 %copy-start.1 = (bf16[2,4096,256]{2,1,0:T(8,128)(2,1)S(1)}, bf16[2,4096,256]{2,1,0:T(8,128)(2,1)}, u32[]{:S(2)}) copy-start(bf16[2,4096,256]{2,1,0:T(8,128)(2,1)} %param.16) | copy-start | bytes 12582916
  48.4 8.5 %copy-start = (bf16[2,1024,1024]{2,1,0:T(8,128)(2,1)S(1)}, bf16[2,1024,1024]{2,1,0:T(8,128)(2,1)}, u32[]{:S(2)}) copy-start(bf16[2,1024,1024]{2,1,0:T(8,128)(2,1)} %param.17) | copy-start | bytes 12582916
where the time goes:
time: 77.1 us; the launch traced here: 76.7 us
  waiting for transfers between devices  27.8 us (36%)
  blocking collectives  25.5 us (33%)
  starting transfers between devices  10.8 us (14%)
  matrix products  8.68 us (11%)
  other arithmetic  3.25 us (4%)
    all_to_all x1, waiting for transfers between devices, on_device(): lax.all_to_all(send_rows, 'ep', split_axis=0, concat_axis=0, tiled=True)  24.8 us
    all_to_all x1, blocking collectives, on_device(): lax.all_to_all(partial_value.reshape(ep_count, capacity, partial_value.sh...  18.2 us
    all_gather x1, blocking collectives, expert_block(): lax.all_gather(activation, 'tp', axis=2, tiled=True)  7.33 us
    all_to_all x1, starting transfers between devices, on_device(): lax.all_to_all(send_weights, 'ep', split_axis=0, concat_axis=0, tiled=True)  7.28 us
    all_to_all x1, starting transfers between devices, on_device(): lax.all_to_all(send_rows, 'ep', split_axis=0, concat_axis=0, tiled=True)  3.56 us
    dot_general x1, matrix products, expert_block(): jnp.einsum('rd,edh->erh', token_rows, w_gate, preferred_element_type=jnp....  3.04 us
    all_to_all x1, waiting for transfers between devices, on_device(): lax.all_to_all(send_weights, 'ep', split_axis=0, concat_axis=0, tiled=True)  2.97 us
    dot_general x1, matrix products, on_device(): jnp.einsum('psr,rd->psd', dispatch.astype(jnp.bfloat16), normed, preferre...  2.44 us
  transfers between devices with their start and end apart: 2, of which 2 were waited for; matrix products, arithmetic and copies ran while one was open for 5% of the time, Pallas kernels for 0%

commit v1 on v0

v1 whole, which is shorter than its diff:
```python
import jax
import jax.numpy as jnp
from jax import lax
from jax.experimental import pallas as pl
from jax.experimental.pallas import tpu as pltpu
from jax.sharding import PartitionSpec as P

EPG = 8
EPS = 1e-06
LANES = 128
ANY = pl.BlockSpec(memory_space=pl.ANY)
BF16 = jnp.bfloat16
F32 = jnp.float32


def split3(value):
    high = value.astype(BF16)
    rest = value - high.astype(F32)
    mid = rest.astype(BF16)
    low = (rest - mid.astype(F32)).astype(BF16)
    return high, mid, low


def half_copies(sources, target, sems, which):
    half = target.shape[2]
    start = pl.multiple_of(which * half, LANES)
    return [
        pltpu.make_async_copy(
            source.at[e, pl.ds(start, half), :], target.at[e, m], sems.at[e, m]
        )
        for e in range(target.shape[0])
        for m, source in enumerate(sources)
    ]


def dispatch_kernel(*refs):
    sources, weights, (send, slots, first), targets = refs[:6], refs[6:8], refs[8:11], refs[11:17]
    sems, weight_sems = refs[17:]
    core = lax.axis_index("tp") % 2
    copies = [
        pltpu.make_async_copy(source, target, sems.at[n])
        for n, (source, target) in enumerate(zip(sources, targets))
    ]
    weight_copies = half_copies(weights, first, weight_sems, core)
    for copy in copies + weight_copies:
        copy.start()
    for copy in copies:
        copy.wait()
    hidden, gain, group, inner, group_prob, expert_prob = targets
    peers, capacity, width = send.shape
    tokens, features = hidden.shape
    groups = slots.shape[0] // capacity
    half = width - LANES
    group_row = group[...]
    strict = (
        lax.broadcasted_iota(jnp.int32, (tokens, tokens), 0)
        < lax.broadcasted_iota(jnp.int32, (tokens, tokens), 1)
    ).astype(BF16)
    slot = lax.broadcasted_iota(jnp.int32, (capacity, tokens), 0)
    one_hot = []
    for g in range(groups):
        member = group_row == g
        flags = jnp.broadcast_to(member.astype(F32), (capacity, tokens)).astype(BF16)
        rank = jnp.dot(flags, strict, preferred_element_type=F32).astype(jnp.int32)
        one_hot.append(((rank == slot) & member).astype(F32))
    picked = jnp.concatenate(one_hot, axis=0).astype(BF16)
    slots[...] = picked
    scaled = expert_prob[...] * group_prob[...]
    expert = lax.broadcasted_iota(jnp.int32, (EPG, tokens), 0)
    weight = jnp.zeros((EPG, tokens), F32)
    for k in range(inner.shape[0]):
        weight += jnp.where(inner[k : k + 1, :] == expert, scaled[k : k + 1, :], 0.0)
    terms = [term.astype(F32) for term in split3(weight)]
    terms.append(jnp.zeros((LANES - 3 * EPG, tokens), F32))
    table = jnp.concatenate(terms, axis=0).astype(BF16)
    rows_weight = lax.dot_general(
        picked, table, (((1,), (1,)), ((), ())), preferred_element_type=F32
    ).astype(BF16)
    wide = hidden[...].astype(F32)
    scale = lax.rsqrt(jnp.sum(wide * wide, axis=-1, keepdims=True) / features + EPS)
    start = pl.multiple_of(core * half, LANES)
    mine = hidden[:, pl.ds(start, half)].astype(F32)
    normed = (mine * scale * gain[:, pl.ds(start, half)]).astype(BF16)
    rows = jnp.dot(picked, normed, preferred_element_type=F32).astype(BF16)
    for p in range(peers):
        g = p * groups // peers
        send[p, :, :half] = rows[g * capacity : (g + 1) * capacity, :]
        send[p, :, half:] = rows_weight[g * capacity : (g + 1) * capacity, :]
    for copy in weight_copies:
        copy.wait()


def first_half_kernel(rows, first, w_gate, w_up, partial, second, sems):
    copies = half_copies((w_gate, w_up), second, sems, 1 - lax.axis_index("tp") % 2)
    for copy in copies:
        copy.start()
    value = rows[:, : first.shape[2]]
    for e in range(first.shape[0]):
        for m in range(2):
            partial[e, m] = jnp.dot(value, first[e, m], preferred_element_type=F32)
    for copy in copies:
        copy.wait()


def second_half_kernel(rows, other, partial, second, w_down, act, down, sem):
    copy = pltpu.make_async_copy(w_down, down, sem)
    copy.start()
    experts, _, half, _ = second.shape
    value = other[:, :half]
    terms = rows[:, half:].astype(F32)
    owners = EPG // experts
    start = (lax.axis_index("ep") % owners) * experts
    lane = lax.broadcasted_iota(jnp.int32, terms.shape, 1)
    for e in range(experts):
        gate = partial[e, 0] + jnp.dot(value, second[e, 0], preferred_element_type=F32)
        up = partial[e, 1] + jnp.dot(value, second[e, 1], preferred_element_type=F32)
        chosen = (lane % EPG == start + e) & (lane < 3 * EPG)
        weight = jnp.sum(jnp.where(chosen, terms, 0.0), axis=-1, keepdims=True)
        act[e] = (gate / (1.0 + jnp.exp(-gate)) * up * weight).astype(BF16)
    copy.wait()


def combine_kernel(returned, slots, out):
    peers, capacity, width = returned.shape
    groups = slots.shape[0] // capacity
    owners = peers // groups
    parts = []
    for g in range(groups):
        parts += [slots[g * capacity : (g + 1) * capacity, :]] * owners
    spread = jnp.concatenate(parts, axis=0)
    value = returned[...].reshape(peers * capacity, width)
    out[...] = lax.dot_general(
        spread, value, (((0,), (0,)), ((), ())), preferred_element_type=F32
    ).astype(BF16)


def down_kernel(act, w_down, sums):
    total = jnp.dot(act[0], w_down[0], preferred_element_type=F32)
    for e in range(1, w_down.shape[0]):
        total += jnp.dot(act[e], w_down[e], preferred_element_type=F32)
    sums[...] = total.astype(BF16)


def kernel_call(body, out_shape, args, stream=(), scratch=(), flops=0, limit=16):
    placed = [pltpu.with_memory_space_constraint(value, pltpu.VMEM) for value in args]
    placed += [pltpu.with_memory_space_constraint(value, pltpu.HBM) for value in stream]
    return pl.pallas_call(
        body,
        out_shape=out_shape,
        in_specs=[pl.BlockSpec(memory_space=pltpu.VMEM)] * len(args) + [ANY] * len(stream),
        scratch_shapes=scratch,
        compiler_params=pltpu.CompilerParams(vmem_limit_bytes=limit * 2**20),
        cost_estimate=pl.CostEstimate(flops=flops, transcendentals=0, bytes_accessed=0),
    )(*placed)


def on_device(
    hidden_in, norm_gain, group_ids, inner_ids, group_prob, expert_prob, w_gate, w_up, w_down
):
    ep_count = lax.axis_size("ep")
    tp_count = lax.axis_size("tp")
    local_count, features, hidden_cols = w_gate.shape
    tokens = hidden_in.shape[0]
    groups = local_count * ep_count // EPG
    capacity = tokens // 2
    rows_count = ep_count * capacity
    half = features // 2
    width = half + LANES
    shape = pltpu.VMEM
    small = (
        hidden_in,
        norm_gain[None, :],
        group_ids[None, :],
        inner_ids.T,
        group_prob[None, :],
        expert_prob.T,
    )
    half_shape = (local_count, 2, half, hidden_cols)
    half_sems = pltpu.SemaphoreType.DMA(half_shape[:2])
    send, slots, first = kernel_call(
        dispatch_kernel,
        (
            shape((ep_count, capacity, width), BF16),
            shape((groups * capacity, tokens), BF16),
            shape(half_shape, BF16),
        ),
        (),
        small + (w_gate, w_up),
        [pltpu.VMEM(value.shape, value.dtype) for value in small]
        + [pltpu.SemaphoreType.DMA((len(small),)), half_sems],
    )
    got = lax.all_to_all(send, "ep", split_axis=0, concat_axis=0, tiled=True)
    rows = got.reshape(rows_count, width)
    swap = [(t, t ^ 1) for t in range(tp_count)]
    other = lax.ppermute(rows, "tp", swap)
    flops = rows_count * half * hidden_cols * local_count * 4
    partial, second = kernel_call(
        first_half_kernel,
        (
            shape((local_count, 2, rows_count, hidden_cols), F32),
            shape(half_shape, BF16),
        ),
        (rows, first),
        (w_gate, w_up),
        [half_sems],
        flops,
    )
    act, w_down = kernel_call(
        second_half_kernel,
        (
            shape((local_count, rows_count, hidden_cols), BF16),
            shape(w_down.shape, BF16),
        ),
        (rows, other, partial, second),
        (w_down,),
        [pltpu.SemaphoreType.DMA],
        flops,
    )
    gathered = lax.all_gather(act, "tp", axis=2, tiled=True)
    out_cols = w_down.shape[2]
    sums = kernel_call(
        down_kernel,
        shape((rows_count, out_cols), BF16),
        (gathered, w_down),
    )
    returned = lax.all_to_all(
        sums.reshape(ep_count, capacity, out_cols),
        "ep",
        split_axis=0,
        concat_axis=0,
        tiled=True,
    )
    return kernel_call(
        combine_kernel,
        jax.ShapeDtypeStruct((tokens, out_cols), BF16),
        (returned, slots),
    )


def solution(mesh):
    placed = (
        P("ep", None),
        P(),
        P("ep"),
        P("ep", None),
        P("ep"),
        P("ep", None),
        P("ep", None, "tp"),
        P("ep", None, "tp"),
        P("ep", None, "tp"),
    )
    return jax.shard_map(
        on_device, mesh=mesh, in_specs=placed, out_specs=P("ep", "tp"), check_vma=False
    )
```

time: 77.1 us -> 51.8 us (0.67)
  waiting for transfers between devices: 27.8 us -> 0.01 us
  blocking collectives: 25.5 us -> 42.6 us
  starting transfers between devices: 10.8 us -> 0.01 us
  Pallas kernels: 0 us -> 8.96 us
  matrix products: 8.68 us -> 0 us
  other arithmetic: 3.25 us -> 0 us
    all_to_all x2 -> x0, waiting for transfers between devices: 27.8 us -> none  [the longest x1 24.8 us: on_device(): lax.all_to_all(send_rows, 'ep', split_axis=0, concat_axis=0, tiled=True)]
    all_to_all x1 -> x2, blocking collectives: 18.2 us -> 35.2 us  [the longest x1 23 us: on_device(): got = lax.all_to_all(send, 'ep', split_axis=0, concat_axis=0, tiled=True)]
    all_to_all x2 -> x0, starting transfers between devices: 10.8 us -> none  [the longest x1 7.28 us: on_device(): lax.all_to_all(send_weights, 'ep', split_axis=0, concat_axis=0, tiled=True)]
    pallas_call x0 -> x5, Pallas kernels: none -> 8.96 us  [kernel_call(): pl.pallas_call(body, out_shape=out_shape, in_specs=[pl.BlockSpec(memory_s...]
    dot_general x6 -> x0, matrix products: 8.68 us -> none  [the longest x1 3.04 us: expert_block(): jnp.einsum('rd,edh->erh', token_rows, w_gate, preferred_element_type=jnp....]
    mul x2 -> x0, other arithmetic: 1.35 us -> none  [the longest x1 0.69 us: on_device(): scaled = group_prob[:, None] * expert_prob]
    reduce_sum x2 -> x0, other arithmetic: 1.12 us -> none  [the longest x1 1.11 us: on_device(): jnp.mean(widened * widened, axis=-1, keepdims=True) + EPS]
  transfers between devices with their start and end apart: 2 -> 1, of which waited for: 2 -> 0; matrix products, arithmetic and copies ran while one was open for 5% -> 0% of each run, Pallas kernels for 0% -> 5%
where the time goes in v1:
time: 51.8 us; the launch traced here: 51.6 us
  blocking collectives  42.6 us (82%)
  Pallas kernels  8.96 us (17%)
    all_to_all x1, blocking collectives, on_device(): got = lax.all_to_all(send, 'ep', split_axis=0, concat_axis=0, tiled=True)  23 us
    all_to_all x1, blocking collectives, on_device(): lax.all_to_all(sums.reshape(ep_count, capacity, out_cols), 'ep', split_ax...  12.1 us
    pallas_call x5, Pallas kernels, kernel_call(): pl.pallas_call(body, out_shape=out_shape, in_specs=[pl.BlockSpec(memory_s...  8.96 us
    all_gather x1, blocking collectives, on_device(): gathered = lax.all_gather(act, 'tp', axis=2, tiled=True)  7.44 us
  transfers between devices with their start and end apart: 1, of which 0 were waited for; matrix products, arithmetic and copies ran while one was open for 0% of the time, Pallas kernels for 5%

profile of v1, /device:TPU:0, one launch (start us, length us, event | category | flops | bytes accessed | tf_op | source)
XLA Modules:
  0.0 51.6 jit_solution(13692254103899909772)
XLA Ops:
  0.0 2.4 %shard_map.91 = (bf16[8,16,2176]{2,1,0:T(8,128)(2,1)S(1)}, bf16[32,32]{1,0:T(8,128)(2,1)S(1)}, bf16[2,2,2048,256]{3,2,1,0:T(8,128)(2,1)S(1)}) custom-call(bf16[32,4096]{1,0:T(8,128)(2,1)} %refs_0_.1, f32[1,4096]{1,0:T(1,128)} %bitcast.11, s32[1,32]{1,0:T(1,128)} %bitcast.14, s32[4,32]{1,0:T(4,128)} %bitcast.12, f32[1,32]{1,0:T(1,128)} %bitcast.15, ...), custom_call_target="tpu_custom_call" | custom-call | tf_op jit(solution)/shard_map/pallas_call | solution.py:147
  2.4 23.0 %all_to_all.10 = bf16[8,16,2176]{2,1,0:T(8,128)(2,1)S(1)} all-to-all(bf16[8,16,2176]{2,1,0:T(8,128)(2,1)S(1)} %get-tuple-element.12), channel_id=1, replica_groups=mesh['ep'=8,'tp'=4] {'ep'}, dimensions={0} | all-to-all | bytes 1114112 | tf_op jit(solution)/shard_map/all_to_all | solution.py:192
  25.5 0.0 collective-permute-start
  25.5 2.8 %shard_map.92 = (f32[2,2,128,256]{3,2,1,0:T(8,128)S(1)}, bf16[2,2,2048,256]{3,2,1,0:T(8,128)(2,1)S(1)}) custom-call(bf16[128,2176]{1,0:T(8,128)(2,1)S(1)} %bitcast.8, bf16[2,2,2048,256]{3,2,1,0:T(8,128)(2,1)S(1)} %get-tuple-element.13.first, bf16[2,4096,256]{2,1,0:T(8,128)(2,1)} %w_gate.1, bf16[2,4096,256]{2,1,0:T(8,128)(2,1)} %w_up.1), custom_call_target="tpu_custom_call" | custom-call | flops 536870912 | tf_op jit(solution)/shard_map/pallas_call | solution.py:147
  28.2 0.0 collective-permute-done.other
  28.3 2.2 %shard_map.93 = (bf16[2,128,256]{2,1,0:T(8,128)(2,1)S(1)}, bf16[2,1024,1024]{2,1,0:T(8,128)(2,1)S(1)}) custom-call(bf16[128,2176]{1,0:T(8,128)(2,1)S(1)} %bitcast.9, bf16[128,2176]{1,0:T(8,128)(2,1)S(1)} %collective-permute-done.other, f32[2,2,128,256]{3,2,1,0:T(8,128)S(1)} %get-tuple-element.14.partial, ...), custom_call_target="tpu_custom_call" | custom-call | flops 536870912 | tf_op jit(solution)/shard_map/pallas_call | solution.py:147
  30.5 7.4 %all_gather.3.act = bf16[2,128,1024]{2,1,0:T(8,128)(2,1)S(1)} all-gather(bf16[2,128,256]{2,1,0:T(8,128)(2,1)S(1)} %get-tuple-element.16), channel_id=1, replica_groups=mesh['ep'=8,'tp'=4] {'tp'}, dimensions={2}, use_global_device_ids=true | all-gather | bytes 655360 | tf_op jit(solution)/shard_map/all_gather | solution.py:219
  37.9 0.7 %shard_map.94 = bf16[128,1024]{1,0:T(8,128)(2,1)S(1)} custom-call(bf16[2,128,1024]{2,1,0:T(8,128)(2,1)S(1)} %all_gather.3.act, bf16[2,1024,1024]{2,1,0:T(8,128)(2,1)S(1)} %get-tuple-element.17.w_down), custom_call_target="tpu_custom_call" | custom-call | tf_op jit(solution)/shard_map/pallas_call | solution.py:147
  38.6 12.1 %all_to_all.11.returned = bf16[8,16,1024]{2,1,0:T(8,128)(2,1)S(1)} all-to-all(bf16[8,16,1024]{2,1,0:T(8,128)(2,1)S(1)} %bitcast.10), channel_id=1, replica_groups=mesh['ep'=8,'tp'=4] {'ep'}, dimensions={0} | all-to-all | bytes 524288 | tf_op jit(solution)/shard_map/all_to_all | solution.py:226
  50.8 0.8 %shard_map.95 = bf16[32,1024]{1,0:T(8,128)(2,1)} custom-call(bf16[8,16,1024]{2,1,0:T(8,128)(2,1)S(1)} %all_to_all.11.returned, bf16[32,32]{1,0:T(8,128)(2,1)S(1)} %get-tuple-element.18.slots), custom_call_target="tpu_custom_call" | custom-call | tf_op jit(solution)/shard_map/pallas_call | solution.py:147
Async XLA Ops:
  25.5 2.8 %collective-permute-start = (bf16[128,2176]{1,0:T(8,128)(2,1)S(1)}, bf16[128,2176]{1,0:T(8,128)(2,1)S(1)}, u32[]{:S(2)}, u32[]{:S(2)}) collective-permute-start(bf16[128,2176]{1,0:T(8,128)(2,1)S(1)} %bitcast.7), channel_id=1, source_target_pairs={{0,1},{1,0},{2,3},{3,2},{4,5},{5,4},{6,7},{7,6},{8,9},{9,8},{10,11... | collective-permute-start | bytes 1671176 | tf_op jit(solution)/shard_map/ppermute | solution.py:195

commit v2 on v1

--- a/solution.py
+++ b/solution.py
@@ -1,3 +1,5 @@
+import functools
+
 import jax
 import jax.numpy as jnp
 from jax import lax
@@ -21,28 +23,14 @@
     return high, mid, low
 
 
-def half_copies(sources, target, sems, which):
-    half = target.shape[2]
-    start = pl.multiple_of(which * half, LANES)
-    return [
-        pltpu.make_async_copy(
-            source.at[e, pl.ds(start, half), :], target.at[e, m], sems.at[e, m]
-        )
-        for e in range(target.shape[0])
-        for m, source in enumerate(sources)
-    ]
-
-
 def dispatch_kernel(*refs):
-    sources, weights, (send, slots, first), targets = refs[:6], refs[6:8], refs[8:11], refs[11:17]
-    sems, weight_sems = refs[17:]
+    sources, (send, slots), targets, sems = refs[:6], refs[6:8], refs[8:14], refs[14]
     core = lax.axis_index("tp") % 2
     copies = [
         pltpu.make_async_copy(source, target, sems.at[n])
         for n, (source, target) in enumerate(zip(sources, targets))
     ]
-    weight_copies = half_copies(weights, first, weight_sems, core)
-    for copy in copies + weight_copies:
+    for copy in copies:
         copy.start()
     for copy in copies:
         copy.wait()
@@ -86,38 +74,35 @@
         g = p * groups // peers
         send[p, :, :half] = rows[g * capacity : (g + 1) * capacity, :]
         send[p, :, half:] = rows_weight[g * capacity : (g + 1) * capacity, :]
-    for copy in weight_copies:
-        copy.wait()
-
-
-def first_half_kernel(rows, first, w_gate, w_up, partial, second, sems):
-    copies = half_copies((w_gate, w_up), second, sems, 1 - lax.axis_index("tp") % 2)
-    for copy in copies:
-        copy.start()
-    value = rows[:, : first.shape[2]]
-    for e in range(first.shape[0]):
-        for m in range(2):
-            partial[e, m] = jnp.dot(value, first[e, m], preferred_element_type=F32)
-    for copy in copies:
-        copy.wait()
-
-
-def second_half_kernel(rows, other, partial, second, w_down, act, down, sem):
-    copy = pltpu.make_async_copy(w_down, down, sem)
-    copy.start()
-    experts, _, half, _ = second.shape
+
+
+def first_half_kernel(rows, w_gate, w_up, partial):
+    half = w_gate.shape[1] // 2
+    start = pl.multiple_of(lax.axis_index("tp") % 2 * half, LANES)
+    value = rows[:, :half]
+    for e in range(w_gate.shape[0]):
+        for m, source in enumerate((w_gate, w_up)):
+            weight = source[e, pl.ds(start, half), :]
+            partial[e, m] = jnp.dot(value, weight, preferred_element_type=F32)
+
+
+def second_half_kernel(rows, other, partial, w_gate, w_up, act):
+    experts = w_gate.shape[0]
+    half = w_gate.shape[1] // 2
+    start = pl.multiple_of((1 - lax.axis_index("tp") % 2) * half, LANES)
     value = other[:, :half]
     terms = rows[:, half:].astype(F32)
     owners = EPG // experts
-    start = (lax.axis_index("ep") % owners) * experts
+    first = (lax.axis_index("ep") % owners) * experts
     lane = lax.broadcasted_iota(jnp.int32, terms.shape, 1)
     for e in range(experts):
-        gate = partial[e, 0] + jnp.dot(value, second[e, 0], preferred_element_type=F32)
-        up = partial[e, 1] + jnp.dot(value, second[e, 1], preferred_element_type=F32)
-        chosen = (lane % EPG == start + e) & (lane < 3 * EPG)
+        gate_weight = w_gate[e, pl.ds(start, half), :]
+        up_weight = w_up[e, pl.ds(start, half), :]
+        gate = partial[e, 0] + jnp.dot(value, gate_weight, preferred_element_type=F32)
+        up = partial[e, 1] + jnp.dot(value, up_weight, preferred_element_type=F32)
+        chosen = (lane % EPG == first + e) & (lane < 3 * EPG)
         weight = jnp.sum(jnp.where(chosen, terms, 0.0), axis=-1, keepdims=True)
         act[e] = (gate / (1.0 + jnp.exp(-gate)) * up * weight).astype(BF16)
-    copy.wait()
 
 
 def combine_kernel(returned, slots, out):
@@ -134,11 +119,20 @@
     ).astype(BF16)
 
 
-def down_kernel(act, w_down, sums):
-    total = jnp.dot(act[0], w_down[0], preferred_element_type=F32)
-    for e in range(1, w_down.shape[0]):
-        total += jnp.dot(act[e], w_down[e], preferred_element_type=F32)
-    sums[...] = total.astype(BF16)
+def down_kernel(*refs, steps, base):
+    acts, w_down, out = refs[: len(steps)], refs[len(steps)], refs[-1]
+    tp_count = lax.axis_size("tp")
+    me = lax.axis_index("tp")
+    cols = acts[0].shape[2]
+    total = refs[len(steps) + 1][...] if base else None
+    for act, (row, core) in zip(acts, steps):
+        owner = (me + tp_count - 2 * row) % tp_count
+        owner = owner + core * (1 - 2 * (owner % 2))
+        start = pl.multiple_of(owner * cols, LANES)
+        for e in range(w_down.shape[0]):
+            part = jnp.dot(act[e], w_down[e, pl.ds(start, cols), :], preferred_element_type=F32)
+            total = part if total is None else total + part
+    out[...] = total.astype(out.dtype)
 
 
 def kernel_call(body, out_shape, args, stream=(), scratch=(), flops=0, limit=16):
@@ -175,56 +169,57 @@
         group_prob[None, :],
         expert_prob.T,
     )
-    half_shape = (local_count, 2, half, hidden_cols)
-    half_sems = pltpu.SemaphoreType.DMA(half_shape[:2])
-    send, slots, first = kernel_call(
+    send, slots = kernel_call(
         dispatch_kernel,
         (
             shape((ep_count, capacity, width), BF16),
             shape((groups * capacity, tokens), BF16),
-            shape(half_shape, BF16),
         ),
         (),
-        small + (w_gate, w_up),
+        small,
         [pltpu.VMEM(value.shape, value.dtype) for value in small]
-        + [pltpu.SemaphoreType.DMA((len(small),)), half_sems],
+        + [pltpu.SemaphoreType.DMA((len(small),))],
+        flops=10**10,
     )
     got = lax.all_to_all(send, "ep", split_axis=0, concat_axis=0, tiled=True)
     rows = got.reshape(rows_count, width)
     swap = [(t, t ^ 1) for t in range(tp_count)]
     other = lax.ppermute(rows, "tp", swap)
     flops = rows_count * half * hidden_cols * local_count * 4
-    partial, second = kernel_call(
+    partial = kernel_call(
         first_half_kernel,
-        (
-            shape((local_count, 2, rows_count, hidden_cols), F32),
-            shape(half_shape, BF16),
-        ),
-        (rows, first),
-        (w_gate, w_up),
-        [half_sems],
-        flops,
-    )
-    act, w_down = kernel_call(
+        shape((local_count, 2, rows_count, hidden_cols), F32),
+        (rows, w_gate, w_up),
+        flops=flops,
+    )
+    act = kernel_call(
         second_half_kernel,
-        (
-            shape((local_count, rows_count, hidden_cols), BF16),
-            shape(w_down.shape, BF16),
-        ),
-        (rows, other, partial, second),
-        (w_down,),
-        [pltpu.SemaphoreType.DMA],
-        flops,
-    )
-    gathered = lax.all_gather(act, "tp", axis=2, tiled=True)
+        shape((local_count, rows_count, hidden_cols), BF16),
+        (rows, other, partial, w_gate, w_up),
+        flops=flops,
+    )
     out_cols = w_down.shape[2]
+    rings = [
+        [(t, (t + 2 * d) % tp_count) for t in range(tp_count)] for d in range(1, tp_count // 2)
+    ]
+    far = [lax.ppermute(act, "tp", ring) for ring in rings]
+    near = lax.ppermute(act, "tp", swap)
     sums = kernel_call(
-        down_kernel,
-        shape((rows_count, out_cols), BF16),
-        (gathered, w_down),
-    )
+        functools.partial(down_kernel, steps=((0, 0), (0, 1)), base=False),
+        shape((rows_count, out_cols), F32),
+        (act, near, w_down),
+        flops=10**8,
+    )
+    steps = tuple((d + 1, core) for d in range(len(far)) for core in range(2))
+    if steps:
+        parts = [value for each in far for value in (each, lax.ppermute(each, "tp", swap))]
+        sums = kernel_call(
+            functools.partial(down_kernel, steps=steps, base=True),
+            shape((rows_count, out_cols), BF16),
+            (*parts, w_down, sums),
+        )
     returned = lax.all_to_all(
-        sums.reshape(ep_count, capacity, out_cols),
+        sums.astype(BF16).reshape(ep_count, capacity, out_cols),
         "ep",
         split_axis=0,
         concat_axis=0,

time: 51.8 us -> 47.9 us (0.925)
  blocking collectives: 42.6 us -> 35.2 us
  waiting for transfers between devices: 0.01 us -> 6.1 us
  Pallas kernels: 8.96 us -> 4.68 us
  starting transfers between devices: 0.01 us -> 1.59 us
    all_gather x1 -> x0, blocking collectives: 7.44 us -> none  [on_device(): gathered = lax.all_gather(act, 'tp', axis=2, tiled=True)]
    ppermute x0 -> x3, waiting for transfers between devices: none -> 4.89 us  [the longest x1 4.01 us: on_device(): far = [lax.ppermute(act, 'tp', ring) for ring in rings]]
    pallas_call x5 -> x6, Pallas kernels: 8.96 us -> 4.68 us  [kernel_call(): pl.pallas_call(body, out_shape=out_shape, in_specs=[pl.BlockSpec(memory_s...]
    ppermute x0 -> x3, starting transfers between devices: none -> 1.59 us  [the longest x1 1.58 us: on_device(): far = [lax.ppermute(act, 'tp', ring) for ring in rings]]
    ppermute x1, waiting for transfers between devices: 0.01 us -> 1.21 us  [on_device(): other = lax.ppermute(rows, 'tp', swap)]
  transfers between devices with their start and end apart: 1 -> 4, of which waited for: 0 -> 3; matrix products, arithmetic and copies ran while one was open for 0% -> 0% of each run, Pallas kernels for 5% -> 2%
where the time goes in v2:
time: 47.9 us; the launch traced here: 47.7 us
  blocking collectives  35.2 us (73%)
  waiting for transfers between devices  6.1 us (13%)
  Pallas kernels  4.68 us (10%)
  starting transfers between devices  1.59 us (3%)
    all_to_all x1, blocking collectives, on_device(): got = lax.all_to_all(send, 'ep', split_axis=0, concat_axis=0, tiled=True)  23.3 us
    all_to_all x1, blocking collectives, on_device(): lax.all_to_all(sums.astype(BF16).reshape(ep_count, capacity, out_cols), '...  11.9 us
    pallas_call x6, Pallas kernels, kernel_call(): pl.pallas_call(body, out_shape=out_shape, in_specs=[pl.BlockSpec(memory_s...  4.68 us
    ppermute x1, waiting for transfers between devices, on_device(): far = [lax.ppermute(act, 'tp', ring) for ring in rings]  4.01 us
    ppermute x1, starting transfers between devices, on_device(): far = [lax.ppermute(act, 'tp', ring) for ring in rings]  1.58 us
    ppermute x1, waiting for transfers between devices, on_device(): other = lax.ppermute(rows, 'tp', swap)  1.21 us
  transfers between devices with their start and end apart: 4, of which 3 were waited for; matrix products, arithmetic and copies ran while one was open for 0% of the time, Pallas kernels for 2%

profile of v2, /device:TPU:0, one launch (start us, length us, event | category | flops | bytes accessed | tf_op | source)
XLA Modules:
  0.0 47.7 jit_solution(18333863847995402153)
XLA Ops:
  0.0 0.0 copy-start.1
  0.0 0.0 copy-start.2
  0.0 1.5 %shard_map.91 = (bf16[8,16,2176]{2,1,0:T(8,128)(2,1)S(1)}, bf16[32,32]{1,0:T(8,128)(2,1)S(1)}) custom-call(bf16[32,4096]{1,0:T(8,128)(2,1)} %refs_0_.1, f32[1,4096]{1,0:T(1,128)} %bitcast.11, s32[1,32]{1,0:T(1,128)} %bitcast.14, s32[4,32]{1,0:T(4,128)} %bitcast.12, f32[1,32]{1,0:T(1,128)} %bitcast.15, f32[4,32]{1,0:T(4,128)} %bitcast.13), custom_call_target="tpu_custom_call" | custom-call | flops 10000000000 | tf_op jit(solution)/shard_map/pallas_call | solution.py:141
  1.5 23.3 %all_to_all.10 = bf16[8,16,2176]{2,1,0:T(8,128)(2,1)S(1)} all-to-all(bf16[8,16,2176]{2,1,0:T(8,128)(2,1)S(1)} %get-tuple-element.7), channel_id=1, replica_groups=mesh['ep'=8,'tp'=4] {'ep'}, dimensions={0} | all-to-all | bytes 1114112 | tf_op jit(solution)/shard_map/all_to_all | solution.py:184
  24.8 0.0 collective-permute-start
  24.8 0.0 copy-done.1
  24.8 0.0 copy-done.2
  24.8 0.7 %shard_map.92.partial = f32[2,2,128,256]{3,2,1,0:T(8,128)S(1)} custom-call(bf16[128,2176]{1,0:T(8,128)(2,1)S(1)} %bitcast.8, bf16[2,4096,256]{2,1,0:T(8,128)(2,1)S(1)} %copy-done.1, bf16[2,4096,256]{2,1,0:T(8,128)(2,1)S(1)} %copy-done.2), custom_call_target="tpu_custom_call" | custom-call | flops 536870912 | tf_op jit(solution)/shard_map/pallas_call | solution.py:141
  25.5 0.0 copy-start
  25.5 1.2 %collective-permute-done.other = bf16[128,2176]{1,0:T(8,128)(2,1)S(1)} collective-permute-done((bf16[128,2176]{1,0:T(8,128)(2,1)S(1)}, bf16[128,2176]{1,0:T(8,128)(2,1)S(1)}, u32[]{:S(2)}, u32[]{:S(2)}) %collective-permute-start) | collective-permute-done | bytes 557088 | tf_op jit(solution)/shard_map/ppermute | solution.py:187
  26.8 0.7 %shard_map.93.refs_0_ = bf16[2,128,256]{2,1,0:T(8,128)(2,1)S(1)} custom-call(bf16[128,2176]{1,0:T(8,128)(2,1)S(1)} %bitcast.9, bf16[128,2176]{1,0:T(8,128)(2,1)S(1)} %collective-permute-done.other, f32[2,2,128,256]{3,2,1,0:T(8,128)S(1)} %shard_map.92.partial, bf16[2,4096,256]{2,1,0:T(8,128)(2,1)S(1)} %copy-done.1, bf16[2,4096,256]{2,1,0:T(8,128)(2,1)S(1)} %copy-done.2), custom_call_target="tpu_custom_call" | custom-call | flops 536870912 | tf_op jit(solution)/shard_map/pallas_call | solution.py:141
  27.5 1.6 %collective-permute-start.1 = (bf16[2,128,256]{2,1,0:T(8,128)(2,1)S(1)}, bf16[2,128,256]{2,1,0:T(8,128)(2,1)S(1)}, u32[]{:S(2)}, u32[]{:S(2)}) collective-permute-start(bf16[2,128,256]{2,1,0:T(8,128)(2,1)S(1)} %shard_map.93.refs_0_), channel_id=1, source_target_pairs={{0,2},{1,3},{2,0},{3,1},{4,6},{5,7},{6,4},{7,5},{8,10},{9,11},{10,... | collective-permute-start | bytes 393224 | tf_op jit(solution)/shard_map/ppermute | solution.py:205
  29.1 0.0 collective-permute-start.3
  29.1 4.0 %collective-permute-done.1.refs_0_ = bf16[2,128,256]{2,1,0:T(8,128)(2,1)S(1)} collective-permute-done((bf16[2,128,256]{2,1,0:T(8,128)(2,1)S(1)}, bf16[2,128,256]{2,1,0:T(8,128)(2,1)S(1)}, u32[]{:S(2)}, u32[]{:S(2)}) %collective-permute-start.1) | collective-permute-done | bytes 131104 | tf_op jit(solution)/shard_map/ppermute | solution.py:205
  33.1 0.0 collective-permute-start.2
  33.1 0.0 collective-permute-done.3.refs_1_
  33.1 0.0 copy-done
  33.1 0.5 shard_map.94.refs_3_
  33.6 0.9 %collective-permute-done.2.refs_1_ = bf16[2,128,256]{2,1,0:T(8,128)(2,1)S(1)} collective-permute-done((bf16[2,128,256]{2,1,0:T(8,128)(2,1)S(1)}, bf16[2,128,256]{2,1,0:T(8,128)(2,1)S(1)}, u32[]{:S(2)}, u32[]{:S(2)}) %collective-permute-start.2) | collective-permute-done | bytes 131104 | tf_op jit(solution)/shard_map/ppermute | solution.py:215
  34.5 0.4 shard_map.95
  34.9 11.9 %all_to_all.11.returned = bf16[8,16,1024]{2,1,0:T(8,128)(2,1)S(1)} all-to-all(bf16[8,16,1024]{2,1,0:T(8,128)(2,1)S(1)} %bitcast.10), channel_id=1, replica_groups=mesh['ep'=8,'tp'=4] {'ep'}, dimensions={0} | all-to-all | bytes 524288 | tf_op jit(solution)/shard_map/all_to_all | solution.py:221
  46.8 0.8 %shard_map.96 = bf16[32,1024]{1,0:T(8,128)(2,1)} custom-call(bf16[8,16,1024]{2,1,0:T(8,128)(2,1)S(1)} %all_to_all.11.returned, bf16[32,32]{1,0:T(8,128)(2,1)S(1)} %get-tuple-element.8.slots), custom_call_target="tpu_custom_call" | custom-call | tf_op jit(solution)/shard_map/pallas_call | solution.py:141
Async XLA Ops:
  0.0 24.8 %copy-start.1 = (bf16[2,4096,256]{2,1,0:T(8,128)(2,1)S(1)}, bf16[2,4096,256]{2,1,0:T(8,128)(2,1)}, u32[]{:S(2)}) copy-start(bf16[2,4096,256]{2,1,0:T(8,128)(2,1)} %w_gate.3) | copy-start | bytes 12582916
  0.0 24.8 %copy-start.2 = (bf16[2,4096,256]{2,1,0:T(8,128)(2,1)S(1)}, bf16[2,4096,256]{2,1,0:T(8,128)(2,1)}, u32[]{:S(2)}) copy-start(bf16[2,4096,256]{2,1,0:T(8,128)(2,1)} %w_up.3) | copy-start | bytes 12582916
  24.8 2.0 %collective-permute-start = (bf16[128,2176]{1,0:T(8,128)(2,1)S(1)}, bf16[128,2176]{1,0:T(8,128)(2,1)S(1)}, u32[]{:S(2)}, u32[]{:S(2)}) collective-permute-start(bf16[128,2176]{1,0:T(8,128)(2,1)S(1)} %bitcast.7), channel_id=1, source_target_pairs={{0,1},{1,0},{2,3},{3,2},{4,5},{5,4},{6,7},{7,6},{8,9},{9,8},{10,11... | collective-permute-start | bytes 1671176 | tf_op jit(solution)/shard_map/ppermute | solution.py:187
  25.5 7.6 %copy-start = (bf16[2,1024,1024]{2,1,0:T(8,128)(2,1)S(1)}, bf16[2,1024,1024]{2,1,0:T(8,128)(2,1)}, u32[]{:S(2)}) copy-start(bf16[2,1024,1024]{2,1,0:T(8,128)(2,1)} %refs_2_.3) | copy-start | bytes 12582916
  27.5 5.6 %collective-permute-start.1 = (bf16[2,128,256]{2,1,0:T(8,128)(2,1)S(1)}, bf16[2,128,256]{2,1,0:T(8,128)(2,1)S(1)}, u32[]{:S(2)}, u32[]{:S(2)}) collective-permute-start(bf16[2,128,256]{2,1,0:T(8,128)(2,1)S(1)} %shard_map.93.refs_0_), channel_id=1, source_target_pairs={{0,2},{1,3},{2,0},{3,1},{4,6},{5,7},{6,4},{7,5},{8,10},{9,11},{10,... | collective-permute-start | bytes 393224 | tf_op jit(solution)/shard_map/ppermute | solution.py:205
  29.1 4.0 %collective-permute-start.3 = (bf16[2,128,256]{2,1,0:T(8,128)(2,1)S(1)}, bf16[2,128,256]{2,1,0:T(8,128)(2,1)S(1)}, u32[]{:S(2)}, u32[]{:S(2)}) collective-permute-start(bf16[2,128,256]{2,1,0:T(8,128)(2,1)S(1)} %shard_map.93.refs_0_), channel_id=1, source_target_pairs={{0,1},{1,0},{2,3},{3,2},{4,5},{5,4},{6,7},{7,6},{8,9},{9,8},{10,11... | collective-permute-start | bytes 393224 | tf_op jit(solution)/shard_map/ppermute | solution.py:206
  33.1 1.3 %collective-permute-start.2 = (bf16[2,128,256]{2,1,0:T(8,128)(2,1)S(1)}, bf16[2,128,256]{2,1,0:T(8,128)(2,1)S(1)}, u32[]{:S(2)}, u32[]{:S(2)}) collective-permute-start(bf16[2,128,256]{2,1,0:T(8,128)(2,1)S(1)} %collective-permute-done.1.refs_0_), channel_id=1, source_target_pairs={{0,1},{1,0},{2,3},{3,2},{4,5},{5,4},{6,7},{7,6},{8,9},{9,8},{10,11... | collective-permute-start | bytes 393224 | tf_op jit(solution)/shard_map/ppermute | solution.py:215
